TPU v7x, 32 devices: a whole 2x2x4 slice. The times are simulated.
32 devices in a mesh: rep: 2 (over y), fs: 4 (over z), tp: 4 (over x, core).
Axes of the slice: x: 2, y: 2, z: 4, core: 2. Of those that a mesh axis runs over, the one named last changes fastest.
Arguments:
- out_grad: bfloat16 [2048, 2048], P(('rep', 'fs'), 'tp'), may hold values from -6 to 6
- gate_lin: bfloat16 [2048, 5632], P(('rep', 'fs'), 'tp'), may hold values from -6 to 6
- up_lin: bfloat16 [2048, 5632], P(('rep', 'fs'), 'tp'), may hold values from -6 to 6
- conv_weight: bfloat16 [3, 5632], replicated, may hold values from -3.5 to 3.5
- gate_weight: bfloat16 [2048, 5632], P('fs', 'tp'), may hold values from -0.125 to 0.125
- up_weight: bfloat16 [2048, 5632], P('fs', 'tp'), may hold values from -0.125 to 0.125
- down_weight: bfloat16 [5632, 2048], P('tp', 'fs'), may hold values from -0.078125 to 0.078125
Outputs:
- input_grad: bfloat16 [2048, 2048], P(('rep', 'fs'), 'tp')
- conv_grad: float32 [3, 5632], replicated
All inputs are finite; a program needn't handle non-finite values.
Results may differ from a plain program's by a relative error of at most 0.015.
Values may be sent and summed in bfloat16 or wider, within the bound.
A program may use at most 64 MiB of HBM per device.

v0:
```python
import math
import jax
import jax.numpy as jnp
from jax import lax
from jax.sharding import PartitionSpec as P


def extended(value, sides, width):
    for axis, dim in sides:
        peers, length = (lax.axis_size(axis), value.shape[dim])
        up = [(i, (i + 1) % peers) for i in range(peers - 1)]
        down = [(j, i) for i, j in up]
        last = lax.slice_in_dim(value, length - width, length, axis=dim)
        leading = lax.slice_in_dim(value, 0, width, axis=dim)
        before = lax.ppermute(last, axis, up)
        after = lax.ppermute(leading, axis, down)
        value = jnp.concatenate([before, value, after], axis=dim)
    return value


def gelu_parts(gate):
    normal_cdf = 0.5 * (1.0 + jax.scipy.special.erf(gate * (1.0 / math.sqrt(2.0))))
    density = jnp.exp(-0.5 * gate * gate) * (1.0 / math.sqrt(2.0 * math.pi))
    return (gate * normal_cdf, normal_cdf + gate * density)


def local(out_grad, gate_lin, up_lin, conv_weight, gate_weight, up_weight, down_weight):
    conv_full = conv_weight.astype(jnp.float32)
    column_count = gate_lin.shape[1]
    column_start = lax.axis_index("tp") * column_count
    conv_taps = lax.dynamic_slice_in_dim(conv_full, column_start, column_count, 1)
    grad_rows = lax.all_gather(out_grad, "tp", axis=1, tiled=True)
    act_grad = lax.dot_general(
        grad_rows,
        lax.all_gather(down_weight, "fs", axis=1, tiled=True),
        (((1,), (1,)), ((), ())),
        preferred_element_type=jnp.float32,
    )
    linear_mid = extended(gate_lin, (("fs", 0),), 1).astype(jnp.float32)
    gate = (
        conv_taps[0] * linear_mid[:-2]
        + conv_taps[1] * linear_mid[1:-1]
        + conv_taps[2] * linear_mid[2:]
    )
    gelu_value, gelu_slope = gelu_parts(gate)
    gate_grad = act_grad * up_lin.astype(jnp.float32) * gelu_slope
    grad_ext = extended(gate_grad.astype(jnp.bfloat16), (("fs", 0),), 1).astype(gate_grad.dtype)
    up_grad = (act_grad * gelu_value).astype(jnp.bfloat16)
    own_grad = grad_ext[1:-1]
    linear_grad = (
        conv_taps[0] * grad_ext[2:] + conv_taps[1] * own_grad + conv_taps[2] * grad_ext[:-2]
    ).astype(jnp.bfloat16)
    local_conv = jnp.stack(
        [
            jnp.sum(own_grad * linear_mid[:-2], axis=0),
            jnp.sum(own_grad * linear_mid[1:-1], axis=0),
            jnp.sum(own_grad * linear_mid[2:], axis=0),
        ]
    )
    product = lax.dot_general(
        linear_grad,
        lax.all_gather(gate_weight, "fs", axis=0, tiled=True),
        (((1,), (1,)), ((), ())),
        preferred_element_type=jnp.float32,
    )
    product = product + lax.dot_general(
        up_grad,
        lax.all_gather(up_weight, "fs", axis=0, tiled=True),
        (((1,), (1,)), ((), ())),
        preferred_element_type=jnp.float32,
    )
    input_grad = lax.psum_scatter(
        product.astype(jnp.bfloat16), "tp", scatter_dimension=1, tiled=True
    )
    summed_conv = lax.psum(local_conv, ("rep", "fs"))
    conv_grad = lax.all_gather(summed_conv, "tp", axis=1, tiled=True)
    return (input_grad, conv_grad)


def solution(mesh):
    return jax.shard_map(
        local,
        mesh=mesh,
        in_specs=(
            P(("rep", "fs"), "tp"),
            P(("rep", "fs"), "tp"),
            P(("rep", "fs"), "tp"),
            P(),
            P("fs", "tp"),
            P("fs", "tp"),
            P("tp", "fs"),
        ),
        out_specs=(P(("rep", "fs"), "tp"), P()),
        check_vma=False,
    )
```

profile of v0, /device:TPU:0, one launch (start us, length us, event | category | flops | bytes accessed | tf_op | source)
XLA Modules:
  0.0 404.9 jit_solution(1864692760127615159)
XLA Ops:
  7.2 0.0 all-gather.5.cloned.1.call-start
  7.2 0.7 all-gather.5.cloned.1.call-update
  7.9 0.0 all-gather.7.cloned.1.call-start
  7.9 0.7 all-gather.7.cloned.1.call-update
  8.6 0.0 copy-start
  8.7 0.0 all-gather.9.cloned.1.call-start
  8.7 0.7 all-gather.9.cloned.1.call-update
  9.4 0.0 all-gather.11.cloned.1.call-start
  9.4 0.5 all-gather.11.cloned.1.call-update
  10.0 0.0 copy-start.1
  10.0 0.0 reduce-scatter.2.cloned.1.call-start
  10.0 0.0 copy-done
  10.1 5.1 %collective-permute-start = (bf16[1,1408]{1,0:T(2,128)(2,1)S(1)}, bf16[1,1408]{1,0:T(2,128)(2,1)S(1)}, u32[]{:S(2)}, u32[]{:S(2)}) collective-permute-start(bf16[1,1408]{1,0:T(2,128)(2,1)S(1)} %get-tuple-element.12), channel_id=1, source_target_pairs={{0,4},{4,8},{8,12},{1,5},{5,9},{9,13},{2,6},{6,10},{10,14},{3,7},{... | collective-permute-start | bytes 8456 | tf_op jit(solution)/shard_map/ppermute | solution.py:15
  15.2 1.3 collective-permute-start.1
  16.5 0.7 dynamic-slice_convert_fusion
  17.2 0.1 slice_reduce_fusion.2
  17.2 0.0 collective-permute-done
  17.2 3.4 collective-permute-done.1
  20.7 0.2 maximum_convert_fusion
  20.8 8.2 %all-gather.5.cloned.1.call-done = bf16[256,2048]{1,0:T(8,128)(2,1)} async-done(((bf16[256,512]{1,0:T(8,128)(2,1)}), bf16[256,2048]{1,0:T(8,128)(2,1)}) %all-gather.5.cloned.1.call-update) | async-done | bytes 1048592 | tf_op jit(solution)/shard_map/all_gather | solution.py:32
  29.0 108.3 %all-gather.7.cloned.1.call-done = bf16[1408,2048]{1,0:T(8,128)(2,1)} async-done(((bf16[1408,512]{1,0:T(8,128)(2,1)}), bf16[1408,2048]{1,0:T(8,128)(2,1)}) %all-gather.7.cloned.1.call-update) | async-done | bytes 5767184 | tf_op jit(solution)/shard_map/all_gather | solution.py:35
  137.3 0.0 copy-done.1
  137.3 7.2 %fusion.6 = (bf16[256,1408]{1,0:T(8,128)(2,1)S(1)}, f32[256,1408]{1,0:T(8,128)}, f32[256,1408]{1,0:T(8,128)}) fusion(bf16[256,1408]{1,0:T(8,128)(2,1)S(1)} %copy-done.1, f32[258,1408]{1,0:T(8,128)S(1)} %maximum_convert_fusion, f32[1408]{0:T(1024)S(1)} %get-tuple-element.7, f32[1408]{0:T(1024)S(1)} %get-tuple-element.6, f32[1408]{0:T(1024)S(1)} %get-tuple-element.5, ...), kind=kOutput, calls=%fused_computation.8 | convolution fusion | flops 1482522624 | bytes 15483392 | tf_op jit(solution)/shard_map/dot_general | solution.py:33
  144.5 1.3 collective-permute-start.2
  145.8 1.3 collective-permute-start.3
  147.1 0.0 collective-permute-done.2
  147.1 4.4 %collective-permute-done.3 = bf16[1,1408]{1,0:T(2,128)(2,1)S(1)} collective-permute-done((bf16[1,1408]{1,0:T(2,128)(2,1)S(1)}, bf16[1,1408]{1,0:T(2,128)(2,1)S(1)}, u32[]{:S(2)}, u32[]{:S(2)}) %collective-permute-start.3) | collective-permute-done | bytes 2848 | tf_op jit(solution)/shard_map/ppermute | solution.py:16
  151.5 0.2 maximum_convert_fusion.1
  151.7 92.3 %all-gather.9.cloned.1.call-done = bf16[2048,1408]{1,0:T(8,128)(2,1)} async-done(((bf16[512,1408]{1,0:T(8,128)(2,1)}), bf16[2048,1408]{1,0:T(8,128)(2,1)}) %all-gather.9.cloned.1.call-update) | async-done | bytes 5767184 | tf_op jit(solution)/shard_map/all_gather | solution.py:62
  244.0 6.0 %fusion.10 = f32[256,2048]{1,0:T(8,128)} fusion(bf16[2048,1408]{1,0:T(8,128)(2,1)} %all-gather.9.cloned.1.call-done, f32[258,1408]{1,0:T(8,128)S(1)} %maximum_convert_fusion.1, f32[1408]{0:T(1024)S(1)} %get-tuple-element.7, f32[1408]{0:T(1024)S(1)} %get-tuple-element.6, f32[1408]{0:T(1024)S(1)} %get-tuple-element.5), kind=kOutput, calls=%fused_computation.22 | convolution fusion | flops 1478557696 | bytes 12214272 | tf_op jit(solution)/shard_map/dot_general | solution.py:60
  249.9 100.4 %all-gather.11.cloned.1.call-done = bf16[2048,1408]{1,0:T(8,128)(2,1)} async-done(((bf16[512,1408]{1,0:T(8,128)(2,1)}), bf16[2048,1408]{1,0:T(8,128)(2,1)}) %all-gather.11.cloned.1.call-update) | async-done | bytes 5767184 | tf_op jit(solution)/shard_map/all_gather | solution.py:68
  350.3 6.9 %fusion = bf16[256,2048]{1,0:T(8,128)(2,1)} fusion(f32[256,2048]{1,0:T(8,128)} %fusion.10, bf16[2048,1408]{1,0:T(8,128)(2,1)} %all-gather.11.cloned.1.call-done, f32[256,1408]{1,0:T(8,128)} %get-tuple-element.14, f32[256,1408]{1,0:T(8,128)} %get-tuple-element.9), kind=kOutput, calls=%fused_computation.1 | convolution fusion | flops 1479606272 | bytes 11796480 | tf_op jit(solution)/shard_map/dot_general | solution.py:66
  357.2 0.0 reduce-scatter.2.cloned.1.call-update
  357.3 0.6 multiply_reduce_fusion.2
  357.9 34.5 %psum.7 = f32[3,1408]{1,0:T(4,128)S(1)} all-reduce(f32[3,1408]{1,0:T(4,128)S(1)} %pad_maximum_fusion), channel_id=1, replica_groups=mesh['rep'=2,'fs'=4,'tp'=4] {'rep','fs'}, use_global_device_ids=true, to_apply=%region_4.0 | all-reduce | flops 4224 | bytes 33792 | tf_op jit(solution)/shard_map/psum | solution.py:75
  392.4 5.3 %all_gather.19 = f32[3,5632]{1,0:T(4,128)S(1)} all-gather(f32[3,1408]{1,0:T(4,128)S(1)} %psum.7), channel_id=1, replica_groups=mesh['rep'=2,'fs'=4,'tp'=4] {'tp'}, dimensions={1}, use_global_device_ids=true | all-gather | bytes 84480 | tf_op jit(solution)/shard_map/all_gather | solution.py:76
  397.7 0.0 reduce-scatter.2.cloned.1.call-done
  397.7 0.6 copy.10
  (6 shorter events, 0.1 us)
Async XLA Ops:
  7.2 21.8 %all-gather.5.cloned.1.call-start = ((), (), s32[]{:S(2)}) async-start(), calls=%async_computation.1 | async-start | bytes 1310720 | tf_op jit(solution)/shard_map/all_gather | solution.py:32
  7.9 129.4 %all-gather.7.cloned.1.call-start = ((), (), s32[]{:S(2)}) async-start(), calls=%async_computation.2 | async-start | bytes 7208960 | tf_op jit(solution)/shard_map/all_gather | solution.py:35
  8.6 1.4 copy-start
  8.7 235.3 %all-gather.9.cloned.1.call-start = ((), (), s32[]{:S(2)}) async-start(), calls=%async_computation.3 | async-start | bytes 7208960 | tf_op jit(solution)/shard_map/all_gather | solution.py:62
  9.4 340.9 %all-gather.11.cloned.1.call-start = ((), (), s32[]{:S(2)}) async-start(), calls=%async_computation.4 | async-start | bytes 7208960 | tf_op jit(solution)/shard_map/all_gather | solution.py:68
  10.0 127.3 %copy-start.1 = (bf16[256,1408]{1,0:T(8,128)(2,1)S(1)}, bf16[256,1408]{1,0:T(8,128)(2,1)}, u32[]{:S(2)}) copy-start(bf16[256,1408]{1,0:T(8,128)(2,1)} %param.9) | copy-start | bytes 2162692
  10.0 387.7 %reduce-scatter.2.cloned.1.call-start = ((), (), s32[]{:S(2)}) async-start(), calls=%async_computation.5 | async-start | bytes 1310720 | tf_op jit(solution)/shard_map/reduce_scatter | solution.py:72
  10.1 7.2 %collective-permute-start = (bf16[1,1408]{1,0:T(2,128)(2,1)S(1)}, bf16[1,1408]{1,0:T(2,128)(2,1)S(1)}, u32[]{:S(2)}, u32[]{:S(2)}) collective-permute-start(bf16[1,1408]{1,0:T(2,128)(2,1)S(1)} %get-tuple-element.12), channel_id=1, source_target_pairs={{0,4},{4,8},{8,12},{1,5},{5,9},{9,13},{2,6},{6,10},{10,14},{3,7},{... | collective-permute-start | bytes 8456 | tf_op jit(solution)/shard_map/ppermute | solution.py:15
  15.2 5.5 %collective-permute-start.1 = (bf16[1,1408]{1,0:T(2,128)(2,1)S(1)}, bf16[1,1408]{1,0:T(2,128)(2,1)S(1)}, u32[]{:S(2)}, u32[]{:S(2)}) collective-permute-start(bf16[1,1408]{1,0:T(2,128)(2,1)S(1)} %get-tuple-element.13), channel_id=1, source_target_pairs={{4,0},{8,4},{12,8},{5,1},{9,5},{13,9},{6,2},{10,6},{14,10},{7,3},{... | collective-permute-start | bytes 8456 | tf_op jit(solution)/shard_map/ppermute | solution.py:16
  144.5 2.6 collective-permute-start.2
  145.8 5.8 %collective-permute-start.3 = (bf16[1,1408]{1,0:T(2,128)(2,1)S(1)}, bf16[1,1408]{1,0:T(2,128)(2,1)S(1)}, u32[]{:S(2)}, u32[]{:S(2)}) collective-permute-start(bf16[1,1408]{1,0:T(2,128)(2,1)S(1)} %get-tuple-element.11), channel_id=1, source_target_pairs={{4,0},{8,4},{12,8},{5,1},{9,5},{13,9},{6,2},{10,6},{14,10},{7,3},{... | collective-permute-start | bytes 8456 | tf_op jit(solution)/shard_map/ppermute | solution.py:16
Sparse Core Ops, SparseCore 0:
  9.5 19.4 all-gather.4
  30.6 106.6 all-gather.6
  138.9 105.0 all-gather.8
  245.4 104.8 all-gather.10
  357.4 23.0 reduce-scatter.1
where the time goes:
time: 405 us
  waiting for transfers between devices  320 us (79%)
  blocking collectives  39.8 us (10%)
  matrix products  20.1 us (5%)
  between operations  13.9 us (3%)
  starting transfers between devices  9.15 us (2%)
    all_gather x1, waiting for transfers between devices, local(): lax.all_gather(down_weight, 'fs', axis=1, tiled=True)  108 us
    all_gather x1, waiting for transfers between devices, local(): lax.all_gather(up_weight, 'fs', axis=0, tiled=True)  100 us
    all_gather x1, waiting for transfers between devices, local(): lax.all_gather(gate_weight, 'fs', axis=0, tiled=True)  92.3 us
    psum x1, blocking collectives, local(): summed_conv = lax.psum(local_conv, ('rep', 'fs'))  34.5 us
    all_gather x1, waiting for transfers between devices, local(): grad_rows = lax.all_gather(out_grad, 'tp', axis=1, tiled=True)  8.16 us
  transfers between devices with their start and end apart: 9, of which 6 were waited for; matrix products, arithmetic and copies ran while one was open for 4% of the time, Pallas kernels for 0%

commit v1 on v0

--- a/solution.py
+++ b/solution.py
@@ -72,7 +72,9 @@
     input_grad = lax.psum_scatter(
         product.astype(jnp.bfloat16), "tp", scatter_dimension=1, tiled=True
     )
-    summed_conv = lax.psum(local_conv, ("rep", "fs"))
+    summed_conv = local_conv
+    for mesh_axis in ("fs", "rep"):
+        summed_conv = lax.psum(summed_conv, mesh_axis)
     conv_grad = lax.all_gather(summed_conv, "tp", axis=1, tiled=True)
     return (input_grad, conv_grad)
 

time: 405 us -> 395 us (0.975)
  blocking collectives: 39.8 us -> 29.7 us
    psum x1 -> x2, blocking collectives: 34.5 us -> 24.4 us  [local(): summed_conv = lax.psum(summed_conv, mesh_axis)]
where the time goes in v1:
time: 395 us
  waiting for transfers between devices  320 us (81%)
  blocking collectives  29.7 us (8%)
  matrix products  20 us (5%)
  between operations  13.9 us (4%)
  starting transfers between devices  9.15 us (2%)
    all_gather x1, waiting for transfers between devices, local(): lax.all_gather(down_weight, 'fs', axis=1, tiled=True)  108 us
    all_gather x1, waiting for transfers between devices, local(): lax.all_gather(up_weight, 'fs', axis=0, tiled=True)  100 us
    all_gather x1, waiting for transfers between devices, local(): lax.all_gather(gate_weight, 'fs', axis=0, tiled=True)  92.3 us
    psum x2, blocking collectives, local(): summed_conv = lax.psum(summed_conv, mesh_axis)  24.4 us
    all_gather x1, waiting for transfers between devices, local(): grad_rows = lax.all_gather(out_grad, 'tp', axis=1, tiled=True)  8.16 us
  transfers between devices with their start and end apart: 9, of which 6 were waited for; matrix products, arithmetic and copies ran while one was open for 4% of the time, Pallas kernels for 0%

profile of v1, /device:TPU:0, one launch (start us, length us, event | category | flops | bytes accessed | tf_op | source)
XLA Modules:
  0.0 394.8 jit_solution(10878238102943732399)
XLA Ops:
  7.2 0.0 all-gather.5.cloned.1.call-start
  7.2 0.7 all-gather.5.cloned.1.call-update
  7.9 0.0 all-gather.7.cloned.1.call-start
  7.9 0.7 all-gather.7.cloned.1.call-update
  8.6 0.0 copy-start
  8.7 0.0 all-gather.9.cloned.1.call-start
  8.7 0.7 all-gather.9.cloned.1.call-update
  9.4 0.0 all-gather.11.cloned.1.call-start
  9.4 0.5 all-gather.11.cloned.1.call-update
  10.0 0.0 copy-start.1
  10.0 0.0 reduce-scatter.2.cloned.1.call-start
  10.0 0.0 copy-done
  10.1 5.1 %collective-permute-start = (bf16[1,1408]{1,0:T(2,128)(2,1)S(1)}, bf16[1,1408]{1,0:T(2,128)(2,1)S(1)}, u32[]{:S(2)}, u32[]{:S(2)}) collective-permute-start(bf16[1,1408]{1,0:T(2,128)(2,1)S(1)} %get-tuple-element.12), channel_id=1, source_target_pairs={{0,4},{4,8},{8,12},{1,5},{5,9},{9,13},{2,6},{6,10},{10,14},{3,7},{... | collective-permute-start | bytes 8456 | tf_op jit(solution)/shard_map/ppermute | solution.py:15
  15.2 1.3 collective-permute-start.1
  16.5 0.7 dynamic-slice_convert_fusion
  17.2 0.1 slice_reduce_fusion.2
  17.2 0.0 collective-permute-done
  17.2 3.4 collective-permute-done.1
  20.7 0.2 maximum_convert_fusion
  20.8 8.2 %all-gather.5.cloned.1.call-done = bf16[256,2048]{1,0:T(8,128)(2,1)} async-done(((bf16[256,512]{1,0:T(8,128)(2,1)}), bf16[256,2048]{1,0:T(8,128)(2,1)}) %all-gather.5.cloned.1.call-update) | async-done | bytes 1048592 | tf_op jit(solution)/shard_map/all_gather | solution.py:32
  29.0 108.3 %all-gather.7.cloned.1.call-done = bf16[1408,2048]{1,0:T(8,128)(2,1)} async-done(((bf16[1408,512]{1,0:T(8,128)(2,1)}), bf16[1408,2048]{1,0:T(8,128)(2,1)}) %all-gather.7.cloned.1.call-update) | async-done | bytes 5767184 | tf_op jit(solution)/shard_map/all_gather | solution.py:35
  137.3 0.0 copy-done.1
  137.3 7.2 %fusion.6 = (bf16[256,1408]{1,0:T(8,128)(2,1)S(1)}, f32[256,1408]{1,0:T(8,128)}, f32[256,1408]{1,0:T(8,128)}) fusion(bf16[256,1408]{1,0:T(8,128)(2,1)S(1)} %copy-done.1, f32[258,1408]{1,0:T(8,128)S(1)} %maximum_convert_fusion, f32[1408]{0:T(1024)S(1)} %get-tuple-element.7, f32[1408]{0:T(1024)S(1)} %get-tuple-element.6, f32[1408]{0:T(1024)S(1)} %get-tuple-element.5, ...), kind=kOutput, calls=%fused_computation.8 | convolution fusion | flops 1482522624 | bytes 15483392 | tf_op jit(solution)/shard_map/dot_general | solution.py:33
  144.5 1.3 collective-permute-start.2
  145.8 1.3 collective-permute-start.3
  147.1 0.0 collective-permute-done.2
  147.1 4.4 %collective-permute-done.3 = bf16[1,1408]{1,0:T(2,128)(2,1)S(1)} collective-permute-done((bf16[1,1408]{1,0:T(2,128)(2,1)S(1)}, bf16[1,1408]{1,0:T(2,128)(2,1)S(1)}, u32[]{:S(2)}, u32[]{:S(2)}) %collective-permute-start.3) | collective-permute-done | bytes 2848 | tf_op jit(solution)/shard_map/ppermute | solution.py:16
  151.5 0.2 maximum_convert_fusion.1
  151.7 92.3 %all-gather.9.cloned.1.call-done = bf16[2048,1408]{1,0:T(8,128)(2,1)} async-done(((bf16[512,1408]{1,0:T(8,128)(2,1)}), bf16[2048,1408]{1,0:T(8,128)(2,1)}) %all-gather.9.cloned.1.call-update) | async-done | bytes 5767184 | tf_op jit(solution)/shard_map/all_gather | solution.py:62
  244.0 6.0 %fusion.10 = f32[256,2048]{1,0:T(8,128)} fusion(bf16[2048,1408]{1,0:T(8,128)(2,1)} %all-gather.9.cloned.1.call-done, f32[258,1408]{1,0:T(8,128)S(1)} %maximum_convert_fusion.1, f32[1408]{0:T(1024)S(1)} %get-tuple-element.7, f32[1408]{0:T(1024)S(1)} %get-tuple-element.6, f32[1408]{0:T(1024)S(1)} %get-tuple-element.5), kind=kOutput, calls=%fused_computation.22 | convolution fusion | flops 1478557696 | bytes 12214272 | tf_op jit(solution)/shard_map/dot_general | solution.py:60
  249.9 100.4 %all-gather.11.cloned.1.call-done = bf16[2048,1408]{1,0:T(8,128)(2,1)} async-done(((bf16[512,1408]{1,0:T(8,128)(2,1)}), bf16[2048,1408]{1,0:T(8,128)(2,1)}) %all-gather.11.cloned.1.call-update) | async-done | bytes 5767184 | tf_op jit(solution)/shard_map/all_gather | solution.py:68
  350.3 6.9 %fusion = bf16[256,2048]{1,0:T(8,128)(2,1)} fusion(f32[256,2048]{1,0:T(8,128)} %fusion.10, bf16[2048,1408]{1,0:T(8,128)(2,1)} %all-gather.11.cloned.1.call-done, f32[256,1408]{1,0:T(8,128)} %get-tuple-element.14, f32[256,1408]{1,0:T(8,128)} %get-tuple-element.9), kind=kOutput, calls=%fused_computation.1 | convolution fusion | flops 1479606272 | bytes 11796480 | tf_op jit(solution)/shard_map/dot_general | solution.py:66
  357.2 0.0 reduce-scatter.2.cloned.1.call-update
  357.3 0.6 multiply_reduce_fusion.2
  357.9 16.0 %psum.14 = f32[3,1408]{1,0:T(4,128)S(1)} all-reduce(f32[3,1408]{1,0:T(4,128)S(1)} %pad_maximum_fusion), channel_id=1, replica_groups=mesh['rep'=2,'fs'=4,'tp'=4] {'fs'}, use_global_device_ids=true, to_apply=%region_4.0 | all-reduce | flops 4224 | bytes 33792 | tf_op jit(solution)/shard_map/psum | solution.py:77
  374.0 8.4 %psum.15 = f32[3,1408]{1,0:T(4,128)S(1)} all-reduce(f32[3,1408]{1,0:T(4,128)S(1)} %psum.14), channel_id=1, replica_groups=mesh['rep'=2,'fs'=4,'tp'=4] {'rep'}, use_global_device_ids=true, to_apply=%region_5.0 | all-reduce | flops 4224 | bytes 33792 | tf_op jit(solution)/shard_map/psum | solution.py:77
  382.4 5.3 %all_gather.19 = f32[3,5632]{1,0:T(4,128)S(1)} all-gather(f32[3,1408]{1,0:T(4,128)S(1)} %psum.15), channel_id=1, replica_groups=mesh['rep'=2,'fs'=4,'tp'=4] {'tp'}, dimensions={1}, use_global_device_ids=true | all-gather | bytes 84480 | tf_op jit(solution)/shard_map/all_gather | solution.py:78
  387.7 0.0 reduce-scatter.2.cloned.1.call-done
  387.7 0.6 copy.10
  (6 shorter events, 0.1 us)
Async XLA Ops:
  7.2 21.8 %all-gather.5.cloned.1.call-start = ((), (), s32[]{:S(2)}) async-start(), calls=%async_computation.1 | async-start | bytes 1310720 | tf_op jit(solution)/shard_map/all_gather | solution.py:32
  7.9 129.4 %all-gather.7.cloned.1.call-start = ((), (), s32[]{:S(2)}) async-start(), calls=%async_computation.2 | async-start | bytes 7208960 | tf_op jit(solution)/shard_map/all_gather | solution.py:35
  8.6 1.4 copy-start
  8.7 235.3 %all-gather.9.cloned.1.call-start = ((), (), s32[]{:S(2)}) async-start(), calls=%async_computation.3 | async-start | bytes 7208960 | tf_op jit(solution)/shard_map/all_gather | solution.py:62
  9.4 340.9 %all-gather.11.cloned.1.call-start = ((), (), s32[]{:S(2)}) async-start(), calls=%async_computation.4 | async-start | bytes 7208960 | tf_op jit(solution)/shard_map/all_gather | solution.py:68
  10.0 127.3 %copy-start.1 = (bf16[256,1408]{1,0:T(8,128)(2,1)S(1)}, bf16[256,1408]{1,0:T(8,128)(2,1)}, u32[]{:S(2)}) copy-start(bf16[256,1408]{1,0:T(8,128)(2,1)} %param.9) | copy-start | bytes 2162692
  10.0 377.7 %reduce-scatter.2.cloned.1.call-start = ((), (), s32[]{:S(2)}) async-start(), calls=%async_computation.5 | async-start | bytes 1310720 | tf_op jit(solution)/shard_map/reduce_scatter | solution.py:72
  10.1 7.2 %collective-permute-start = (bf16[1,1408]{1,0:T(2,128)(2,1)S(1)}, bf16[1,1408]{1,0:T(2,128)(2,1)S(1)}, u32[]{:S(2)}, u32[]{:S(2)}) collective-permute-start(bf16[1,1408]{1,0:T(2,128)(2,1)S(1)} %get-tuple-element.12), channel_id=1, source_target_pairs={{0,4},{4,8},{8,12},{1,5},{5,9},{9,13},{2,6},{6,10},{10,14},{3,7},{... | collective-permute-start | bytes 8456 | tf_op jit(solution)/shard_map/ppermute | solution.py:15
  15.2 5.5 %collective-permute-start.1 = (bf16[1,1408]{1,0:T(2,128)(2,1)S(1)}, bf16[1,1408]{1,0:T(2,128)(2,1)S(1)}, u32[]{:S(2)}, u32[]{:S(2)}) collective-permute-start(bf16[1,1408]{1,0:T(2,128)(2,1)S(1)} %get-tuple-element.13), channel_id=1, source_target_pairs={{4,0},{8,4},{12,8},{5,1},{9,5},{13,9},{6,2},{10,6},{14,10},{7,3},{... | collective-permute-start | bytes 8456 | tf_op jit(solution)/shard_map/ppermute | solution.py:16
  144.5 2.6 collective-permute-start.2
  145.8 5.8 %collective-permute-start.3 = (bf16[1,1408]{1,0:T(2,128)(2,1)S(1)}, bf16[1,1408]{1,0:T(2,128)(2,1)S(1)}, u32[]{:S(2)}, u32[]{:S(2)}) collective-permute-start(bf16[1,1408]{1,0:T(2,128)(2,1)S(1)} %get-tuple-element.11), channel_id=1, source_target_pairs={{4,0},{8,4},{12,8},{5,1},{9,5},{13,9},{6,2},{10,6},{14,10},{7,3},{... | collective-permute-start | bytes 8456 | tf_op jit(solution)/shard_map/ppermute | solution.py:16
Sparse Core Ops, SparseCore 0:
  9.5 19.4 all-gather.4
  30.6 106.6 all-gather.6
  138.9 105.0 all-gather.8
  245.4 104.8 all-gather.10
  357.4 23.0 reduce-scatter.1
